TPU v7x, 32 devices: a whole 2x2x4 slice. The times are simulated.
32 devices in a mesh: sp: 8 (over z, x), tp: 4 (over y, core).
Axes of the slice: x: 2, y: 2, z: 4, core: 2. Of those that a mesh axis runs over, the one named last changes fastest.
Arguments:
- query_wide: bfloat16 [1024, 1536], P('sp', 'tp'), may hold values from -600 to 600
- query_narrow: bfloat16 [1024, 1024], P('sp', 'tp'), may hold values from -600 to 600
- latent: bfloat16 [1024, 512], P('sp'), may hold values from -6 to 6
- rope_key: bfloat16 [1024, 64], P('sp'), may hold values from -6 to 6
- latent_norm_weight: float32 [512], replicated, may hold values from 0.1 to 1.9
- broad_key_lift: bfloat16 [512, 1024], P(None, 'tp'), may hold values from -0.25 to 0.25
- broad_value_lift: bfloat16 [512, 1024], P(None, 'tp'), may hold values from -0.25 to 0.25
- slim_key_lift: bfloat16 [512, 512], P(None, 'tp'), may hold values from -0.25 to 0.25
- slim_value_lift: bfloat16 [512, 512], P(None, 'tp'), may hold values from -0.25 to 0.25
- out_wide: bfloat16 [1024, 2048], P('tp'), may hold values from -0.4375 to 0.4375
- out_narrow: bfloat16 [512, 2048], P('tp'), may hold values from -0.4375 to 0.4375
- resid: bfloat16 [1024, 2048], P('sp'), may hold values from -20 to 20
- ffn_gain: float32 [2048], replicated, may hold values from 0.1 to 1.9
- group_route: int32 [1024], P('sp'), may hold values from 0 to 7, as said below
- expert_pair: int32 [1024, 2], P('sp'), may hold values from 0 to 3, all different within a row
- group_prob: float32 [1024], P('sp'), may hold values from 0.2 to 1
- expert_prob: float32 [1024, 2], P('sp'), may hold values from 0.05 to 1
- gate_weight: bfloat16 [8, 4, 2048, 512], P('sp', None, None, 'tp'), may hold values from -0.125 to 0.125
- up_weight: bfloat16 [8, 4, 2048, 512], P('sp', None, None, 'tp'), may hold values from -0.125 to 0.125
- down_weight: bfloat16 [8, 4, 512, 2048], P('sp', None, 'tp'), may hold values from -0.25 to 0.25
Outputs:
- mixed: bfloat16 [1024, 2048], P('sp', 'tp')
Inputs may be any that keep to these rules, and one draw needn't show every extreme that they name: `group_route`: of the 128 tokens of one index of sp at most 32 name one group; in every draw one group is named by exactly 32 tokens of every index of sp, and every index of sp names one more group exactly 32 times. `expert_pair`: A token's two experts are different.
All inputs are finite; a program needn't handle non-finite values.
Results may differ from a plain program's by a relative error of at most 0.017.
Values may be sent and summed in bfloat16 or wider, within the bound.
No kernel may reach another device: no remote copies, remote signals or barrier semaphores. Data moves between devices by JAX's collectives and lax.ppermute only.
A program may use at most 128 MiB of HBM per device.

v0:
```python
import math

import jax
import jax.numpy as jnp
from jax import lax
from jax.sharding import PartitionSpec as P

PLAIN_WIDTH_WIDE = 128
PLAIN_WIDTH_SLIM = 64
ROPE = 64
VALUE_WIDTH_WIDE = 128
VALUE_WIDTH_SLIM = 64
EPG = 4


ROPE_BASE = 10000.0
EPSILON = 1e-06
MASKED = -1e30


def rms_scale(values, gain_row):
    widened = values.astype(jnp.float32)
    return (
        widened
        * lax.rsqrt(jnp.mean(widened * widened, axis=-1, keepdims=True) + EPSILON)
        * gain_row
    )


def angles(positions, width):
    frequency = 1.0 / ROPE_BASE ** (jnp.arange(0, width, 2).astype(jnp.float32) / width)
    return positions.astype(jnp.float32)[:, None] * frequency[None, :]


def rotary(values, angle_table):
    half_width = values.shape[-1] // 2
    first_half = values[..., :half_width]
    second = values[..., half_width:]
    return jnp.concatenate(
        [
            first_half * jnp.cos(angle_table) - second * jnp.sin(angle_table),
            second * jnp.cos(angle_table) + first_half * jnp.sin(angle_table),
        ],
        axis=-1,
    )


def split_query(queries, head_count, nope_width, angle_table):
    shaped = queries.reshape(queries.shape[0], head_count, nope_width + ROPE)
    turned = rotary(shaped[..., nope_width:].astype(jnp.float32), angle_table[:, None, :]).astype(
        jnp.bfloat16
    )
    return (shaped[..., :nope_width], turned)


def group_step(
    carry_state, query_pair, key_block, value_block, rot_block, key_pos, query_pos, scale
):
    row_peak, row_total, accum_out = carry_state
    scores = jnp.einsum(
        "thd,khd->htk", query_pair[0], key_block, preferred_element_type=jnp.float32
    )
    scores = scores + jnp.einsum(
        "thd,kd->htk", query_pair[1], rot_block, preferred_element_type=jnp.float32
    )
    scores = jnp.where((query_pos[:, None] >= key_pos[None, :])[None], scores * scale, MASKED)
    new_peak = jnp.maximum(row_peak, jnp.max(scores, axis=-1))
    keep_factor = jnp.exp(row_peak - new_peak)
    weights = jnp.exp(scores - new_peak[:, :, None])
    row_total = row_total * keep_factor + jnp.sum(weights, axis=-1)
    accum_out = accum_out * keep_factor.T[:, :, None] + jnp.einsum(
        "htk,khd->thd",
        weights.astype(jnp.bfloat16),
        value_block,
        preferred_element_type=jnp.float32,
    )
    return (new_peak, row_total, accum_out)


def empty_state(head_count, width, local_tokens):
    return (
        jnp.full((head_count, local_tokens), MASKED, jnp.float32),
        jnp.zeros((head_count, local_tokens), jnp.float32),
        jnp.zeros((local_tokens, head_count, width), jnp.float32),
    )


def finish(carry_state):
    normalized = carry_state[2] / carry_state[1].T[:, :, None]
    return normalized.astype(jnp.bfloat16).reshape(normalized.shape[0], -1)


def project(latent_rows, weight):
    return jnp.dot(latent_rows, weight, preferred_element_type=jnp.float32).astype(jnp.bfloat16)


def body(
    query_wide,
    query_narrow,
    latent,
    rope_key,
    latent_norm_weight,
    broad_key_lift,
    broad_value_lift,
    slim_key_lift,
    slim_value_lift,
    out_wide,
    out_narrow,
    resid,
    ffn_gain,
    group_route,
    expert_pair,
    group_prob,
    expert_prob,
    gate_weight,
    up_weight,
    down_weight,
):
    local_tokens = latent.shape[0]
    offset = lax.axis_index("sp") * local_tokens
    query_pos = offset + jnp.arange(local_tokens, dtype=jnp.int32)
    angle_table = angles(query_pos, ROPE)
    latent_rows = rms_scale(latent, latent_norm_weight).astype(jnp.bfloat16)
    rot_key = rotary(rope_key.astype(jnp.float32), angle_table).astype(jnp.bfloat16)
    heads_wide = query_wide.shape[1] // (PLAIN_WIDTH_WIDE + ROPE)
    heads_narrow = query_narrow.shape[1] // (PLAIN_WIDTH_SLIM + ROPE)
    wide_query = split_query(query_wide, heads_wide, PLAIN_WIDTH_WIDE, angle_table)
    narrow_query = split_query(query_narrow, heads_narrow, PLAIN_WIDTH_SLIM, angle_table)

    def expand(lat_block):
        return (
            project(lat_block, broad_key_lift),
            project(lat_block, broad_value_lift),
            project(lat_block, slim_key_lift),
            project(lat_block, slim_value_lift),
        )

    def attend(carry_state, key_set, key_pos):
        key_w, value_w, key_n, value_n, rot_block = key_set
        block_rows = rot_block.shape[0]
        wide_state = group_step(
            carry_state[0],
            wide_query,
            key_w.reshape(block_rows, heads_wide, PLAIN_WIDTH_WIDE),
            value_w.reshape(block_rows, heads_wide, VALUE_WIDTH_WIDE),
            rot_block,
            key_pos,
            query_pos,
            (PLAIN_WIDTH_WIDE + ROPE) ** (-0.5),
        )
        narrow_state = group_step(
            carry_state[1],
            narrow_query,
            key_n.reshape(block_rows, heads_narrow, PLAIN_WIDTH_SLIM),
            value_n.reshape(block_rows, heads_narrow, VALUE_WIDTH_SLIM),
            rot_block,
            key_pos,
            query_pos,
            (PLAIN_WIDTH_SLIM + ROPE) ** (-0.5),
        )
        return (wide_state, narrow_state)

    start_state = (
        empty_state(heads_wide, VALUE_WIDTH_WIDE, local_tokens),
        empty_state(heads_narrow, VALUE_WIDTH_SLIM, local_tokens),
    )
    pieces = (
        lax.all_gather(latent_rows, "sp", axis=0, tiled=True),
        lax.all_gather(rot_key, "sp", axis=0, tiled=True),
    )
    total_rows = pieces[0].shape[0]
    block_rows = math.gcd(total_rows, 1024)

    def visit_block(block_index, carry_inner):
        block_start = block_index * block_rows
        sliced = tuple(
            (lax.dynamic_slice_in_dim(piece, block_start, block_rows, 0) for piece in pieces)
        )
        key_pos = block_start + jnp.arange(block_rows, dtype=jnp.int32)

        def work_block(running):
            key_set = expand(sliced[0]) + (sliced[1],)
            return attend(running, key_set, key_pos)

        return lax.cond(
            block_start > query_pos[-1], lambda unchanged: unchanged, work_block, carry_inner
        )

    final_state = lax.fori_loop(0, total_rows // block_rows, visit_block, start_state)
    att_wide = finish(final_state[0])
    att_narrow = finish(final_state[1])
    partial_value = jnp.dot(att_wide, out_wide, preferred_element_type=jnp.float32)
    partial_value = partial_value + jnp.dot(
        att_narrow, out_narrow, preferred_element_type=jnp.float32
    )
    model_width = resid.shape[1]
    tp_size = lax.axis_size("tp")
    quarter = model_width // tp_size
    col_start = lax.axis_index("tp") * quarter
    summed = lax.psum(partial_value.astype(jnp.bfloat16), "tp").astype(jnp.float32)
    stream = (resid.astype(jnp.float32) + summed).astype(jnp.bfloat16)
    normed = rms_scale(stream, ffn_gain).astype(jnp.bfloat16)
    stream_cols = lax.dynamic_slice_in_dim(stream, col_start, quarter, 1)
    groups = lax.axis_size("sp")
    capacity = 2 * local_tokens // groups
    share_of = group_prob[:, None] * expert_prob / jnp.sum(expert_prob, axis=1, keepdims=True)
    chosen = (expert_pair[:, :, None] == jnp.arange(EPG, dtype=jnp.int32)[None, None, :]).astype(
        jnp.float32
    )
    combine = jnp.sum(share_of[:, :, None] * chosen, axis=1).astype(jnp.bfloat16)
    member = (group_route[:, None] == jnp.arange(groups, dtype=jnp.int32)[None, :]).astype(
        jnp.int32
    )
    group_rank = jnp.sum(jnp.cumsum(member, axis=0) * member, axis=1) - 1
    slot_index = group_route * capacity + group_rank
    routed_weights = jnp.zeros((groups * capacity, EPG), jnp.bfloat16).at[slot_index].set(combine)
    routed_weights = routed_weights.reshape(groups, capacity, EPG)
    column_rows = lax.dynamic_slice_in_dim(normed, col_start, quarter, 1)
    placed = (
        jnp.zeros((groups * capacity, column_rows.shape[1]), jnp.bfloat16)
        .at[slot_index]
        .set(column_rows)
    )
    joined = lax.all_gather(
        lax.all_to_all(
            placed.reshape(groups, capacity, column_rows.shape[1]),
            "sp",
            split_axis=0,
            concat_axis=0,
            tiled=True,
        ),
        "tp",
        axis=2,
        tiled=True,
    )
    slot_count = joined.shape[0] * joined.shape[1]
    flat_rows = joined.reshape(slot_count, joined.shape[2])
    gate_act = jnp.einsum(
        "rd,edf->ref", flat_rows, gate_weight[0], preferred_element_type=jnp.float32
    )
    up_act = jnp.einsum("rd,edf->ref", flat_rows, up_weight[0], preferred_element_type=jnp.float32)
    scaled = (
        lax.all_to_all(routed_weights, "sp", split_axis=0, concat_axis=0, tiled=True)
        .reshape(slot_count, EPG)
        .astype(jnp.float32)[:, :, None]
    )
    hidden = (jax.nn.silu(gate_act) * up_act * scaled).astype(jnp.bfloat16)
    partials = jnp.einsum("ref,efd->rd", hidden, down_weight[0], preferred_element_type=jnp.float32)
    partials = partials.reshape(joined.shape)
    summed_rows = lax.psum_scatter(
        partials.astype(jnp.bfloat16), "tp", scatter_dimension=2, tiled=True
    )
    returned_rows = lax.all_to_all(summed_rows, "sp", split_axis=0, concat_axis=0, tiled=True)
    moe_rows = returned_rows.reshape(groups * capacity, quarter)[slot_index]
    return (stream_cols.astype(jnp.float32) + moe_rows.astype(jnp.float32)).astype(jnp.bfloat16)


def solution(mesh):
    placed = (
        P("sp", "tp"),
        P("sp", "tp"),
        P("sp", None),
        P("sp", None),
        P(),
        P(None, "tp"),
        P(None, "tp"),
        P(None, "tp"),
        P(None, "tp"),
        P("tp", None),
        P("tp", None),
        P("sp", None),
        P(),
        P("sp"),
        P("sp", None),
        P("sp"),
        P("sp", None),
        P("sp", None, None, "tp"),
        P("sp", None, None, "tp"),
        P("sp", None, "tp", None),
    )
    return jax.shard_map(body, mesh=mesh, in_specs=placed, out_specs=P("sp", "tp"), check_vma=False)
```

profile of v0, /device:TPU:0, one launch (start us, length us, event | category | flops | bytes accessed | tf_op | source)
XLA Modules:
  0.0 180.7 jit_solution(8999266724435186518)
XLA Ops:
  6.5 1.2 fusion.38
  7.7 1.7 fusion.40
  9.4 0.0 all-gather.3.cloned.1.call-update
  9.4 0.0 all-reduce.2.cloned.1.call-start
  9.5 0.7 convert_element_type.130
  10.2 1.0 copy.74
  11.2 1.0 copy.75
  12.2 0.6 slice.38
  13.5 0.7 fusion.48
  14.2 0.2 reduce_window_sum.11
  14.4 0.2 multiply_cosine_fusion
  14.6 28.3 %all_gather.10 = bf16[1024,64]{0,1:T(8,128)(2,1)S(1)} all-gather(bf16[128,64]{0,1:T(8,128)(2,1)S(1)} %pad_maximum_fusion.2), channel_id=1, replica_groups=mesh['sp'=8,'tp'=4] {'sp'}, dimensions={0}, use_global_device_ids=true | all-gather | bytes 147456 | tf_op jit(solution)/shard_map/all_gather | solution.py:169
  43.0 0.6 pad_maximum_fusion
  43.6 9.6 %all-gather.3.cloned.1.call-done = bf16[1024,512]{1,0:T(8,128)(2,1)} async-done(((bf16[128,512]{1,0:T(8,128)(2,1)}), bf16[1024,512]{1,0:T(8,128)(2,1)}) %all-gather.3.cloned.1.call-update) | async-done | bytes 1048592 | tf_op jit(solution)/shard_map/all_gather | solution.py:168
  53.2 7.1 %conditional.1 = (f32[2,128]{1,0:T(2,128)S(1)}, f32[128,2,128]{0,2,1:T(8,128)S(1)}, f32[2,128]{1,0:T(2,128)S(1)}, f32[128,2,64]{0,2,1:T(8,128)S(1)}) conditional(s32[]{:T(128)} %bitcast.13, (s32[128]{0:T(128)S(1)}, s32[1024]{0:T(1024)S(1)}, bf16[1024,512]{1,0:T(8,128)(2,1)}, bf16[512,256]{1,0:T(8,128)(2,1)S(1)}, bf16[128,2,192]{0,2,1:T(8,128)(2,1)S(1)}, ...), branch_computations={%region_1.6_spmd, %region_6.7_spmd} | conditional | flops 1078953472 | bytes 26996452 | solution.py:185
  53.2 0.6 copy-done.6
  53.8 1.7 convolution_convert_fusion.1
  55.5 0.1 copy.76
  55.7 0.4 convolution_bitcast_fusion
  56.0 0.0 copy-start.7
  56.0 0.2 broadcast_compare_fusion
  56.2 0.4 fusion.53
  56.6 0.2 copy-done.1
  56.9 0.5 convolution_convert_fusion.3
  57.4 0.3 convolution_bitcast_fusion.2
  57.7 0.0 copy-start.10
  57.7 0.4 fusion.52
  58.1 0.0 copy-start.5
  58.1 0.3 fusion.9
  58.5 0.2 copy-done.10
  58.6 0.5 convolution_convert_fusion.2
  59.1 0.3 fusion.7
  59.4 0.5 convolution_convert_fusion
  59.9 0.3 fusion.6
  60.4 0.0 copy-start.2
  60.4 1.6 fusion.54
  62.0 1.1 fusion.23
  63.1 0.0 all-reduce.2.cloned.1.call-update
  63.2 0.0 all-gather.5.cloned.1.call-start
  63.2 0.2 select_reduce_fusion
  63.4 0.8 dynamic-slice
  64.2 31.1 %all-reduce.2.cloned.1.call-done = bf16[128,2048]{1,0:T(8,128)(2,1)} async-done(((bf16[128,2048]{1,0:T(8,128)(2,1)}), bf16[128,2048]{1,0:T(8,128)(2,1)}) %all-reduce.2.cloned.1.call-update) | async-done | bytes 524304 | tf_op jit(solution)/shard_map/psum | solution.py:200
  95.3 1.3 multiply_reduce_fusion
  96.6 1.1 convert_element_type.142
  97.7 1.6 scatter_custom_fusion
  99.3 13.6 %all_to_all.15 = bf16[8,32,512]{2,1,0:T(8,128)(2,1)} all-to-all(bf16[8,32,512]{2,1,0:T(8,128)(2,1)S(1)} %bitcast.107), channel_id=1, replica_groups=mesh['sp'=8,'tp'=4] {'sp'}, dimensions={0} | all-to-all | bytes 524288 | tf_op jit(solution)/shard_map/all_to_all | solution.py:225
  112.9 0.0 all-gather.5.cloned.1.call-update
  112.9 0.0 reduce-scatter.2.cloned.1.call-start
  113.1 0.1 copy.77
  113.2 0.9 scatter_custom_fusion.1
  114.1 0.1 copy.78
  114.2 9.7 %all_to_all.16 = bf16[8,32,4]{1,2,0:T(4,128)(2,1)S(1)} all-to-all(bf16[8,32,4]{1,2,0:T(4,128)(2,1)S(1)} %copy.78), channel_id=1, replica_groups=mesh['sp'=8,'tp'=4] {'sp'}, dimensions={0} | all-to-all | bytes 4096 | tf_op jit(solution)/shard_map/all_to_all | solution.py:243
  123.9 0.1 reshape.185
  124.0 4.1 %all-gather.5.cloned.1.call-done = bf16[8,32,2048]{2,1,0:T(8,128)(2,1)} async-done(((bf16[8,32,512]{2,1,0:T(8,128)(2,1)}), bf16[8,32,2048]{2,1,0:T(8,128)(2,1)}) %all-gather.5.cloned.1.call-update) | async-done | bytes 1048592 | tf_op jit(solution)/shard_map/all_gather | solution.py:224
  128.1 2.8 %fusion.27 = f32[256,4,128]{2,0,1:T(8,128)S(1)} fusion(bf16[256,2048,1]{1,0,2:T(8,128)(2,1)} %bitcast.119, bf16[1,4,2048,128]{3,2,1,0:T(8,128)(2,1)} %param.39), kind=kOutput, calls=%fused_computation.49 | convolution fusion | flops 536870912 | bytes 3670016 | tf_op jit(solution)/shard_map/rd,edf->ref/dot_general | solution.py:238
  130.9 0.0 copy-done.16
  130.9 0.7 fusion.35
  131.7 1.7 fusion.22
  133.4 0.0 reduce-scatter.2.cloned.1.call-update
  133.4 24.9 %reduce-scatter.2.cloned.1.call-done = bf16[8,32,512]{2,1,0:T(8,128)(2,1)} async-done(((bf16[8,32,2048]{2,1,0:T(8,128)(2,1)}), bf16[8,32,512]{2,1,0:T(8,128)(2,1)}) %reduce-scatter.2.cloned.1.call-update) | async-done | bytes 262160 | tf_op jit(solution)/shard_map/reduce_scatter | solution.py:250
  158.3 5.5 %all-to-all-start.2 = ((bf16[8,32,512]{2,1,0:T(8,128)(2,1)}), bf16[8,32,512]{2,1,0:T(8,128)(2,1)S(1)}, u32[]{:S(2)}, u32[]{:S(2)}) async-start(bf16[8,32,512]{2,1,0:T(8,128)(2,1)} %reduce-scatter.2.cloned.1.call-done), calls=%async_computation.3 | async-start | bytes 524288 | tf_op jit(solution)/shard_map/all_to_all | solution.py:253
  163.9 8.7 %all-to-all-done.2 = bf16[8,32,512]{2,1,0:T(8,128)(2,1)S(1)} async-done(((bf16[8,32,512]{2,1,0:T(8,128)(2,1)}), bf16[8,32,512]{2,1,0:T(8,128)(2,1)S(1)}, u32[]{:S(2)}, u32[]{:S(2)}) %all-to-all-start.2) | async-done | bytes 262176 | tf_op jit(solution)/shard_map/all_to_all | solution.py:253
  172.6 0.8 gather_fusion
  173.4 0.7 add_convert_fusion.1
  (51 shorter events, 0.3 us)
Async XLA Ops:
  6.5 125.1 %copy-start = (bf16[1,4,128,2048]{3,2,1,0:T(8,128)(2,1)S(1)}, bf16[1,4,128,2048]{3,2,1,0:T(8,128)(2,1)}, u32[]{:S(2)}) copy-start(bf16[1,4,128,2048]{3,2,1,0:T(8,128)(2,1)} %param.41) | copy-start | bytes 6291460
  6.5 46.6 %copy-start.4 = (bf16[512,256]{1,0:T(8,128)(2,1)S(1)}, bf16[512,256]{1,0:T(8,128)(2,1)}, u32[]{:S(2)}) copy-start(bf16[512,256]{1,0:T(8,128)(2,1)} %param.27) | copy-start | bytes 786436
  6.5 46.6 %all-gather.3.cloned.1.call-start = ((), (), s32[]{:S(2)}) async-start(), calls=%async_computation.4 | async-start | bytes 1179648 | tf_op jit(solution)/shard_map/all_gather | solution.py:168
  9.4 85.8 %all-reduce.2.cloned.1.call-start = ((), (), s32[]{:S(2)}) async-start(), calls=%async_computation.5 | async-start | bytes 1048576 | tf_op jit(solution)/shard_map/psum | solution.py:200
  53.2 0.6 copy-start.6
  55.6 1.2 copy-start.1
  55.6 1.2 copy-start.9
  56.0 1.3 copy-start.7
  56.2 1.5 copy-start.8
  57.7 0.9 copy-start.10
  58.1 1.3 copy-start.5
  60.3 1.7 copy-start.3
  60.4 2.9 %copy-start.12 = (s32[128]{0:T(128)S(1)}, s32[128]{0:T(128)}, u32[]{:S(2)}) copy-start(s32[128]{0:T(128)} %param.35) | copy-start | bytes 1540
  60.4 34.9 %copy-start.2 = (bf16[128,2048]{1,0:T(8,128)(2,1)S(1)}, bf16[128,2048]{1,0:T(8,128)(2,1)}, u32[]{:S(2)}) copy-start(bf16[128,2048]{1,0:T(8,128)(2,1)} %param.33) | copy-start | bytes 1572868
  63.2 64.9 %all-gather.5.cloned.1.call-start = ((), (), s32[]{:S(2)}) async-start(), calls=%async_computation.6 | async-start | bytes 1310720 | tf_op jit(solution)/shard_map/all_gather | solution.py:224
  64.2 48.8 %copy-start.11 = (f32[128,2]{0,1:T(2,128)S(1)}, f32[128,2]{0,1:T(2,128)}, u32[]{:S(2)}) copy-start(f32[128,2]{0,1:T(2,128)} %param.38) | copy-start | bytes 3076
  64.2 48.8 %copy-start.14 = (f32[128]{0:T(128)S(1)}, f32[128]{0:T(128)}, u32[]{:S(2)}) copy-start(f32[128]{0:T(128)} %param.37) | copy-start | bytes 1540
  64.2 48.9 %copy-start.13 = (s32[128,2]{0,1:T(2,128)S(1)}, s32[128,2]{0,1:T(2,128)}, u32[]{:S(2)}) copy-start(s32[128,2]{0,1:T(2,128)} %param.36) | copy-start | bytes 3076
  112.9 45.4 %reduce-scatter.2.cloned.1.call-start = ((), (), s32[]{:S(2)}) async-start(), calls=%async_computation.7 | async-start | bytes 1310720 | tf_op jit(solution)/shard_map/reduce_scatter | solution.py:250
  128.1 2.8 %copy-start.15 = (bf16[1,4,2048,128]{3,2,1,0:T(8,128)(2,1)S(1)}, bf16[1,4,2048,128]{3,2,1,0:T(8,128)(2,1)}, u32[]{:S(2)}) copy-start(bf16[1,4,2048,128]{3,2,1,0:T(8,128)(2,1)} %param.40) | copy-start | bytes 6291460
  128.1 2.8 %copy-start.16 = (bf16[8,32,2048]{2,1,0:T(8,128)(2,1)S(1)}, bf16[8,32,2048]{2,1,0:T(8,128)(2,1)}, u32[]{:S(2)}) copy-start(bf16[8,32,2048]{2,1,0:T(8,128)(2,1)} %all-gather.5.cloned.1.call-done) | copy-start | bytes 3145732
  158.3 14.3 %all-to-all-start.2 = ((bf16[8,32,512]{2,1,0:T(8,128)(2,1)}), bf16[8,32,512]{2,1,0:T(8,128)(2,1)S(1)}, u32[]{:S(2)}, u32[]{:S(2)}) async-start(bf16[8,32,512]{2,1,0:T(8,128)(2,1)} %reduce-scatter.2.cloned.1.call-done), calls=%async_computation.3 | async-start | bytes 524288 | tf_op jit(solution)/shard_map/all_to_all | solution.py:253
Sparse Core Ops, SparseCore 0:
  9.5 43.5 all-gather.2
  63.3 31.9 all-reduce.1
  113.1 14.9 all-gather.4
  133.5 24.7 reduce-scatter.1
where the time goes:
time: 181 us
  waiting for transfers between devices  78.5 us (43%)
  blocking collectives  51.6 us (29%)
  between operations  14 us (8%)
  matrix products  13.2 us (7%)
  other arithmetic  10.8 us (6%)
  local copies, waits for them, and re-layouts  6.7 us (4%)
  starting transfers between devices  5.64 us (3%)
    psum x1, waiting for transfers between devices, body(): lax.psum(partial_value.astype(jnp.bfloat16), 'tp').astype(jnp.float32)  31.1 us
    all_gather x1, blocking collectives, body(): lax.all_gather(rot_key, 'sp', axis=0, tiled=True)  28.3 us
    reduce_scatter x1, waiting for transfers between devices, body(): lax.psum_scatter(partials.astype(jnp.bfloat16), 'tp', scatter_dimension=2...  24.9 us
    all_to_all x1, blocking collectives, body(): lax.all_to_all(placed.reshape(groups, capacity, column_rows.shape[1]), 's...  13.6 us
    all_to_all x1, blocking collectives, body(): lax.all_to_all(routed_weights, 'sp', split_axis=0, concat_axis=0, tiled=T...  9.66 us
    all_gather x1, waiting for transfers between devices, body(): lax.all_gather(latent_rows, 'sp', axis=0, tiled=True)  9.58 us
    all_to_all x1, waiting for transfers between devices, body(): lax.all_to_all(summed_rows, 'sp', split_axis=0, concat_axis=0, tiled=True)  8.74 us
    all_to_all x1, starting transfers between devices, body(): lax.all_to_all(summed_rows, 'sp', split_axis=0, concat_axis=0, tiled=True)  5.51 us
  transfers between devices with their start and end apart: 5, of which 5 were waited for; matrix products, arithmetic and copies ran while one was open for 4% of the time, Pallas kernels for 0%

commit v1 on v0

v1 whole, which is shorter than its diff:
```python
import jax
import jax.numpy as jnp
from jax import lax
from jax.experimental import pallas as pl
from jax.experimental.pallas import tpu as pltpu
from jax.sharding import PartitionSpec as P

PLAIN_WIDTH_WIDE = 128
PLAIN_WIDTH_SLIM = 64
ROPE = 64
VALUE_WIDTH_WIDE = 128
VALUE_WIDTH_SLIM = 64
EPG = 4
LANES = 128

ROPE_BASE = 10000.0
EPSILON = 1e-06
MASKED = -1e30

VMEM = pl.BlockSpec(memory_space=pltpu.VMEM)
SMEM = pl.BlockSpec(memory_space=pltpu.SMEM)


def angles(positions, width):
    frequency = 1.0 / ROPE_BASE ** (jnp.arange(0, width, 2).astype(jnp.float32) / width)
    return positions.astype(jnp.float32)[:, None] * frequency[None, :]


def turn(values, cosine, sine):
    half_width = values.shape[-1] // 2
    first_half = values[..., :half_width]
    second = values[..., half_width:]
    return jnp.concatenate(
        [first_half * cosine - second * sine, second * cosine + first_half * sine], axis=-1
    )


def exchange(values, axis, mask):
    size = lax.axis_size(axis)
    return lax.ppermute(values, axis, [(i, i ^ mask) for i in range(size)])


def pack_kernel(latent_ref, rope_ref, gain_ref, cos_ref, sin_ref, meta_ref, out_ref):
    rank = latent_ref.shape[1]
    widened = latent_ref[...].astype(jnp.float32)
    scale = lax.rsqrt(jnp.mean(widened * widened, axis=-1, keepdims=True) + EPSILON)
    out_ref[:, :rank] = (widened * scale * gain_ref[...]).astype(jnp.bfloat16)
    turned = turn(rope_ref[...].astype(jnp.float32), cos_ref[...], sin_ref[...])
    out_ref[:, rank:] = jnp.concatenate([turned, meta_ref[...]], axis=-1).astype(jnp.bfloat16)


def dot_t(a, b):
    return lax.dot_general(a, b, (((1,), (1,)), ((), ())), preferred_element_type=jnp.float32)


def dot(a, b):
    return jnp.dot(a, b, preferred_element_type=jnp.float32)


def attend_body(where_ref, q_ref, mine_ref, other_ref, kw_ref, vw_ref, kn_ref, vn_ref, state, x_bit):
    heads_w = kw_ref.shape[1] // PLAIN_WIDTH_WIDE
    heads_n = kn_ref.shape[1] // PLAIN_WIDTH_SLIM
    blocks, half, width = mine_ref.shape
    tokens = q_ref.shape[1]
    rank = kw_ref.shape[0]
    place = where_ref[0]
    core = where_ref[1]
    step_blocks = min(blocks, 4)
    rows = step_blocks * half
    shift = half.bit_length() - 1
    for start in range(0, blocks, step_blocks):
        lat = jnp.concatenate(
            [
                mine_ref[start : start + step_blocks].reshape(rows, width),
                other_ref[start : start + step_blocks].reshape(rows, width),
            ],
            axis=0,
        )
        flat = lat[:, :rank]
        rot = lat[:, rank:]
        key_w = dot(flat, kw_ref[...]).astype(jnp.bfloat16)
        key_n = dot(flat, kn_ref[...]).astype(jnp.bfloat16)
        val_w = dot(flat, vw_ref[...]).astype(jnp.bfloat16)
        val_n = dot(flat, vn_ref[...]).astype(jnp.bfloat16)
        lane = lax.broadcasted_iota(jnp.int32, (tokens, 2 * rows), 1)
        row = lax.broadcasted_iota(jnp.int32, (tokens, 2 * rows), 0)
        first = lane < rows
        inner = jnp.where(first, lane, lane - rows)
        block = place ^ (2 * (start + (inner >> shift)) + x_bit)
        offset = jnp.where(first, core, 1 - core)
        key_pos = (block * 2 + offset) * half + (inner & (half - 1))
        visible = row + place * tokens >= key_pos
        new_state = []
        for h in range(heads_w + heads_n):
            if h < heads_w:
                keys = key_w[:, h * PLAIN_WIDTH_WIDE : (h + 1) * PLAIN_WIDTH_WIDE]
                values = val_w[:, h * VALUE_WIDTH_WIDE : (h + 1) * VALUE_WIDTH_WIDE]
                scale = (PLAIN_WIDTH_WIDE + ROPE) ** (-0.5)
            else:
                keys = key_n
                values = val_n
                scale = (PLAIN_WIDTH_SLIM + ROPE) ** (-0.5)
            scores = dot_t(q_ref[h], jnp.concatenate([keys, rot], axis=1)) * scale
            scores = jnp.where(visible, scores, MASKED)
            peak = jnp.max(scores, axis=-1, keepdims=True)
            if state is not None:
                peak = jnp.maximum(peak, state[h][0])
            weights = jnp.exp(scores - peak)
            total = jnp.sum(weights, axis=-1, keepdims=True)
            acc = dot(weights.astype(jnp.bfloat16), values)
            if state is not None:
                keep = jnp.exp(state[h][0] - peak)
                total = total + state[h][1] * keep
                acc = acc + state[h][2] * keep
            new_state.append((peak, total, acc))
        state = new_state
    return state


def first_kernel(where_ref, q_ref, mine_ref, other_ref, kw_ref, vw_ref, kn_ref, vn_ref, peak_ref, total_ref, acc_ref):
    state = attend_body(where_ref, q_ref, mine_ref, other_ref, kw_ref, vw_ref, kn_ref, vn_ref, None, 0)
    for h, (peak, total, acc) in enumerate(state):
        peak_ref[h] = jnp.broadcast_to(peak, peak_ref.shape[1:])
        total_ref[h] = jnp.broadcast_to(total, total_ref.shape[1:])
        acc_ref[h] = acc


def second_kernel(
    where_ref, q_ref, mine_ref, other_ref, kw_ref, vw_ref, kn_ref, vn_ref,
    peak_ref, total_ref, acc_ref, ow_ref, on_ref, keep_ref, send_ref,
):
    heads = peak_ref.shape[0]
    heads_w = kw_ref.shape[1] // PLAIN_WIDTH_WIDE
    state = [(peak_ref[h, :, :1], total_ref[h, :, :1], acc_ref[h]) for h in range(heads)]
    state = attend_body(where_ref, q_ref, mine_ref, other_ref, kw_ref, vw_ref, kn_ref, vn_ref, state, 1)
    done = [acc / total for _, total, acc in state]
    att_w = jnp.concatenate(done[:heads_w], axis=1).astype(jnp.bfloat16)
    att_n = jnp.concatenate(
        [
            done[heads_w + h][:, h * VALUE_WIDTH_SLIM : (h + 1) * VALUE_WIDTH_SLIM]
            for h in range(heads - heads_w)
        ],
        axis=1,
    ).astype(jnp.bfloat16)
    core = where_ref[1]
    pieces, _, quarter = keep_ref.shape
    for piece in range(pieces):
        for ref, bit in ((send_ref, 1 - core), (keep_ref, core)):
            cols = pl.ds(pl.multiple_of((2 * piece + bit) * quarter, LANES), quarter)
            ref[piece] = (dot(att_w, ow_ref[:, cols]) + dot(att_n, on_ref[:, cols])).astype(jnp.bfloat16)


def call(kernel, out_shape, n_args, smem=True, flops=0):
    return pl.pallas_call(
        kernel,
        out_shape=out_shape,
        in_specs=([SMEM] if smem else []) + [VMEM] * (n_args - smem),
        out_specs=jax.tree.map(lambda _: VMEM, out_shape),
        cost_estimate=pl.CostEstimate(flops=flops, transcendentals=0, bytes_accessed=0),
        compiler_params=pltpu.CompilerParams(vmem_limit_bytes=56 * 2**20),
    )


def sum_scatter(low, high, first_bit, place):
    size = lax.axis_size("tp")
    bit = first_bit
    while True:
        mine = ((place >> bit) & 1) == 1
        send = jnp.stack([jnp.where(mine, a, b) for a, b in zip(low, high)]).astype(jnp.bfloat16)
        got = exchange(send, "tp", 1 << bit)
        now = [
            jnp.where(mine, b, a).astype(jnp.float32) + got[i].astype(jnp.float32)
            for i, (a, b) in enumerate(zip(low, high))
        ]
        bit += 1
        if (1 << bit) >= size:
            return now[0]
        low, high = now[0::2], now[1::2]


def body(
    query_wide,
    query_narrow,
    latent,
    rope_key,
    latent_norm_weight,
    broad_key_lift,
    broad_value_lift,
    slim_key_lift,
    slim_value_lift,
    out_wide,
    out_narrow,
    resid,
    ffn_gain,
    group_route,
    expert_pair,
    group_prob,
    expert_prob,
    gate_weight,
    up_weight,
    down_weight,
):
    tokens, rank = latent.shape
    groups = lax.axis_size("sp")
    tp_size = lax.axis_size("tp")
    place = lax.axis_index("sp")
    lane_place = lax.axis_index("tp")
    core = lane_place & 1
    half = tokens // 2
    capacity = 2 * tokens // groups
    model_width = resid.shape[1]
    quarter = model_width // tp_size
    f32, bf16 = jnp.float32, jnp.bfloat16

    share_of = group_prob[:, None] * expert_prob / jnp.sum(expert_prob, axis=1, keepdims=True)
    chosen = (expert_pair[:, :, None] == jnp.arange(EPG, dtype=jnp.int32)[None, None, :]).astype(f32)
    combine = jnp.sum(share_of[:, :, None] * chosen, axis=1)
    meta = jnp.concatenate(
        [
            combine,
            group_route.astype(f32)[:, None],
            jnp.zeros((tokens, LANES - ROPE - EPG - 1), f32),
        ],
        axis=1,
    )
    query_pos = place * tokens + jnp.arange(tokens, dtype=jnp.int32)
    angle_table = angles(query_pos, ROPE)
    cosine, sine = jnp.cos(angle_table), jnp.sin(angle_table)
    packed = call(pack_kernel, jax.ShapeDtypeStruct((tokens, rank + LANES), bf16), 6, smem=False)(
        latent, rope_key, latent_norm_weight[None, :], cosine, sine, meta
    )
    halves = packed.reshape(2, half, rank + LANES)
    own_half = jnp.where(core == 1, halves[1], halves[0])
    own_rest = jnp.where(core == 1, halves[0], halves[1])

    strides = list(range(2, groups, 2))
    got = {k: exchange(own_half, "sp", k) for k in reversed(strides)}
    column_got = [got[k] for k in strides]
    column = jnp.stack([own_half] + column_got)
    across = exchange(column, "sp", 1)
    column_rest = exchange(jnp.stack(column_got), "tp", 1)
    column_rest = jnp.concatenate([own_rest[None], column_rest], axis=0)
    across_rest = exchange(across, "tp", 1)

    heads_w = query_wide.shape[1] // (PLAIN_WIDTH_WIDE + ROPE)
    heads_n = query_narrow.shape[1] // (PLAIN_WIDTH_SLIM + ROPE)
    slim_lanes = heads_n * PLAIN_WIDTH_SLIM
    queries = []
    for source, heads, plain in (
        (query_wide, heads_w, PLAIN_WIDTH_WIDE),
        (query_narrow, heads_n, PLAIN_WIDTH_SLIM),
    ):
        for h in range(heads):
            part = source[:, h * (plain + ROPE) : (h + 1) * (plain + ROPE)]
            turned = turn(part[:, plain:].astype(f32), cosine, sine).astype(bf16)
            pieces = [part[:, :plain], turned, jnp.zeros((tokens, LANES - ROPE), bf16)]
            if plain == PLAIN_WIDTH_SLIM:
                before = jnp.zeros((tokens, h * plain), bf16)
                after = jnp.zeros((tokens, slim_lanes - (h + 1) * plain), bf16)
                pieces = [before, pieces[0], after] + pieces[1:]
            queries.append(jnp.concatenate(pieces, axis=1))
    queries = jnp.stack(queries)
    where = jnp.stack([place, core]).astype(jnp.int32)
    heads = heads_w + heads_n
    lifts = (broad_key_lift, broad_value_lift, slim_key_lift, slim_value_lift)
    state_shape = [jax.ShapeDtypeStruct((heads, tokens, LANES), f32)] * 3
    state = call(first_kernel, state_shape, 8, flops=10**9)(where, queries, column, column_rest, *lifts)
    piece_shape = jax.ShapeDtypeStruct((tp_size // 2, tokens, quarter), bf16)
    keep, send = call(second_kernel, [piece_shape] * 2, 13, flops=10**9)(
        where, queries, across, across_rest, *lifts, *state, out_wide, out_narrow
    )

    received = exchange(send, "tp", 1)
    paired = [keep[i].astype(f32) + received[i].astype(f32) for i in range(tp_size // 2)]
    summed = sum_scatter(paired[0::2], paired[1::2], 1, lane_place)
    resid_cols = lax.dynamic_slice_in_dim(resid, lane_place * quarter, quarter, 1)
    stream_cols = (resid_cols.astype(f32) + summed).astype(bf16)

    member = (group_route[:, None] == jnp.arange(groups, dtype=jnp.int32)[None, :]).astype(f32)
    upto = (jnp.arange(tokens)[:, None] >= jnp.arange(tokens)[None, :]).astype(f32)
    rank_of = jnp.sum(jnp.dot(upto, member) * member, axis=1).astype(jnp.int32) - 1
    slot_index = group_route * capacity + rank_of
    slot_hot = (slot_index[None, :] == jnp.arange(groups * capacity, dtype=jnp.int32)[:, None]).astype(bf16)

    first_part = jnp.concatenate([column[:, :, rank + ROPE : rank + ROPE + EPG + 1], across[:, :, rank + ROPE : rank + ROPE + EPG + 1]])
    second_part = jnp.concatenate([column_rest[:, :, rank + ROPE : rank + ROPE + EPG + 1], across_rest[:, :, rank + ROPE : rank + ROPE + EPG + 1]])
    gathered = jnp.where(
        core == 1,
        jnp.concatenate([second_part, first_part], axis=1),
        jnp.concatenate([first_part, second_part], axis=1),
    )
    here = (gathered[:, :, EPG].astype(jnp.int32) == place).astype(f32)
    order_here = jnp.einsum("kt,ut->ku", here, upto).astype(jnp.int32) - 1
    hot_here = (
        (order_here[:, None, :] == jnp.arange(capacity, dtype=jnp.int32)[None, :, None])
        & (here[:, None, :] > 0)
    ).astype(bf16)
    slot_weights = jnp.einsum("kct,kte->kce", hot_here, gathered[:, :, :EPG], preferred_element_type=f32)
    masks = jnp.arange(groups, dtype=jnp.int32)
    stack_of = jnp.where(masks & 1 == 1, groups // 2, 0) + (masks >> 1)
    pick = (stack_of[place ^ masks][:, None] == masks[None, :]).astype(f32)
    slot_weights = jnp.einsum("sk,kce->sce", pick, slot_weights, precision=lax.Precision.HIGHEST)
    slot_weights = slot_weights.reshape(groups * capacity, EPG)

    placed = dot(slot_hot, stream_cols).astype(bf16).reshape(groups, capacity, quarter)
    routed = lax.all_to_all(placed, "sp", split_axis=0, concat_axis=0, tiled=True)
    routed = routed.reshape(groups * capacity, quarter)
    parts = [routed]
    for bit in reversed(range(tp_size.bit_length() - 1)):
        parts = parts + [exchange(part, "tp", 1 << bit) for part in parts]
    masks_of = [0]
    for bit in reversed(range(tp_size.bit_length() - 1)):
        masks_of = masks_of + [m ^ (1 << bit) for m in masks_of]
    by_mask = [parts[masks_of.index(m)] for m in range(tp_size)]
    for bit in range(tp_size.bit_length() - 1):
        set_bit = ((lane_place >> bit) & 1) == 1
        by_mask = [jnp.where(set_bit, by_mask[m ^ (1 << bit)], by_mask[m]) for m in range(tp_size)]
    rows = jnp.concatenate(by_mask, axis=1).astype(f32)
    row_scale = lax.rsqrt(jnp.mean(rows * rows, axis=-1, keepdims=True) + EPSILON)
    normed = (rows * row_scale * ffn_gain).astype(bf16)
    gate_act = jnp.einsum("rd,edf->ref", normed, gate_weight[0], preferred_element_type=f32)
    up_act = jnp.einsum("rd,edf->ref", normed, up_weight[0], preferred_element_type=f32)
    hidden = (jax.nn.silu(gate_act) * up_act * slot_weights[:, :, None]).astype(bf16)
    partials = jnp.einsum("ref,efd->rd", hidden, down_weight[0], preferred_element_type=f32)
    cols = [partials[:, i * quarter : (i + 1) * quarter].astype(bf16) for i in range(tp_size)]
    summed_rows = sum_scatter(cols[0::2], cols[1::2], 0, lane_place).astype(bf16)
    returned = lax.all_to_all(
        summed_rows.reshape(groups, capacity, quarter), "sp", split_axis=0, concat_axis=0, tiled=True
    ).reshape(groups * capacity, quarter)
    moe_rows = lax.dot_general(slot_hot, returned, (((0,), (0,)), ((), ())), preferred_element_type=f32)
    return (stream_cols.astype(f32) + moe_rows).astype(bf16)


def solution(mesh):
    placed = (
        P("sp", "tp"),
        P("sp", "tp"),
        P("sp", None),
        P("sp", None),
        P(),
        P(None, "tp"),
        P(None, "tp"),
        P(None, "tp"),
        P(None, "tp"),
        P("tp", None),
        P("tp", None),
        P("sp", None),
        P(),
        P("sp"),
        P("sp", None),
        P("sp"),
        P("sp", None),
        P("sp", None, None, "tp"),
        P("sp", None, None, "tp"),
        P("sp", None, "tp", None),
    )
    return jax.shard_map(body, mesh=mesh, in_specs=placed, out_specs=P("sp", "tp"), check_vma=False)
```

time: 181 us -> 110 us (0.61)
  waiting for transfers between devices: 78.5 us -> 36.2 us
  blocking collectives: 51.6 us -> 13.2 us
  between operations: 14 us -> 0.22 us
  Pallas kernels: 0 us -> 11.5 us
  starting transfers between devices: 5.64 us -> 16.4 us
  matrix products: 13.2 us -> 8.91 us
  other arithmetic: 10.8 us -> 13.8 us
  local copies, waits for them, and re-layouts: 6.7 us -> 9.02 us
    psum x1 -> x0, waiting for transfers between devices: 31.1 us -> none  [body(): lax.psum(partial_value.astype(jnp.bfloat16), 'tp').astype(jnp.float32)]
    all_gather x1 -> x0, blocking collectives: 28.3 us -> none  [body(): lax.all_gather(rot_key, 'sp', axis=0, tiled=True)]
    ppermute x0 -> x13, waiting for transfers between devices: none -> 27.4 us  [exchange(): return lax.ppermute(values, axis, [(i, i ^ mask) for i in range(size)])]
    reduce_scatter x1 -> x0, waiting for transfers between devices: 24.9 us -> none  [body(): lax.psum_scatter(partials.astype(jnp.bfloat16), 'tp', scatter_dimension=2...]
    all_gather x2 -> x0, waiting for transfers between devices: 13.7 us -> none  [the longest x1 9.58 us: body(): lax.all_gather(latent_rows, 'sp', axis=0, tiled=True)]
    ppermute x0 -> x13, starting transfers between devices: none -> 12.2 us  [exchange(): return lax.ppermute(values, axis, [(i, i ^ mask) for i in range(size)])]
    pallas_call x0 -> x3, Pallas kernels: none -> 11.5 us  [the longest x1 5.6 us: body(): call(second_kernel, [piece_shape] * 2, 13, flops=10 ** 9)]
    all_to_all x2 -> x1, blocking collectives: 23.3 us -> 13.2 us  [body(): lax.all_to_all(summed_rows.reshape(groups, capacity, quarter), 'sp', spli...]
  transfers between devices with their start and end apart: 5 -> 14, of which waited for: 5 -> 10; matrix products, arithmetic and copies ran while one was open for 4% -> 8% of each run, Pallas kernels for 0% -> 4%
where the time goes in v1:
time: 110 us; the launch traced here: 109 us
  waiting for transfers between devices  36.2 us (33%)
  starting transfers between devices  16.4 us (15%)
  other arithmetic  13.8 us (13%)
  blocking collectives  13.2 us (12%)
  Pallas kernels  11.5 us (10%)
  local copies, waits for them, and re-layouts  9.02 us (8%)
  matrix products  8.91 us (8%)
    ppermute x13, waiting for transfers between devices, exchange(): return lax.ppermute(values, axis, [(i, i ^ mask) for i in range(size)])  27.4 us
    all_to_all x1, blocking collectives, body(): lax.all_to_all(summed_rows.reshape(groups, capacity, quarter), 'sp', spli...  13.2 us
    ppermute x13, starting transfers between devices, exchange(): return lax.ppermute(values, axis, [(i, i ^ mask) for i in range(size)])  12.2 us
    all_to_all x1, waiting for transfers between devices, body(): lax.all_to_all(placed, 'sp', split_axis=0, concat_axis=0, tiled=True)  8.79 us
    pallas_call x1, Pallas kernels, body(): call(second_kernel, [piece_shape] * 2, 13, flops=10 ** 9)  5.6 us
    all_to_all x1, starting transfers between devices, body(): lax.all_to_all(placed, 'sp', split_axis=0, concat_axis=0, tiled=True)  4.25 us
    pallas_call x1, Pallas kernels, body(): call(first_kernel, state_shape, 8, flops=10 ** 9)  4.03 us
    unnamed x25, local copies, waits for them, and re-layouts  3.67 us
  transfers between devices with their start and end apart: 14, of which 10 were waited for; matrix products, arithmetic and copies ran while one was open for 8% of the time, Pallas kernels for 4%

profile of v1, /device:TPU:0, one launch (start us, length us, event | category | flops | bytes accessed | tf_op | source)
XLA Modules:
  0.0 109.3 jit_solution(11483989533343513299)
XLA Ops:
  0.0 1.0 fusion.20
  1.0 0.8 add_add_fusion
  1.8 1.4 %copy.53.rope_ref = bf16[128,64]{1,0:T(8,128)(2,1)} copy(bf16[128,64]{0,1:T(8,128)(2,1)} %param.23) | data formatting | bytes 32768 | tf_op args[3]
  3.2 0.7 reduce_sum.36
  3.9 0.7 multiply_divide_fusion
  4.6 0.7 select_reduce_fusion
  5.3 0.1 copy.51
  5.4 0.1 copy.52
  5.6 0.9 slice_convert_fusion.1
  6.5 0.7 maximum_maximum_fusion.meta_ref
  7.2 1.0 fusion.59
  8.2 1.9 %shard_map.190 = bf16[128,640]{1,0:T(8,128)(2,1)} custom-call(bf16[128,512]{1,0:T(8,128)(2,1)} %latent_ref.1, bf16[128,64]{1,0:T(8,128)(2,1)} %copy.53.rope_ref, f32[1,512]{1,0:T(1,128)} %bitcast.104, f32[128,32]{1,0:T(8,128)} %get-tuple-element.47.cos_ref, f32[128,32]{1,0:T(8,128)} %get-tuple-element.48.sin_ref, f32[128,64]{1,0:T(8,128)} %maximum_maximum_fusion.meta_ref), custom_call_target="tpu_custom_call" | custom-call | tf_op jit(solution)/shard_map/pallas_call | solution.py:229
  10.1 0.9 select_bitcast_fusion.2
  11.1 5.1 %collective-permute-start.2 = (bf16[64,640]{1,0:T(8,128)(2,1)S(1)}, bf16[64,640]{1,0:T(8,128)(2,1)S(1)}, u32[]{:S(2)}, u32[]{:S(2)}) collective-permute-start(bf16[64,640]{1,0:T(8,128)(2,1)S(1)} %get-tuple-element.24), channel_id=1, source_target_pairs={{0,24},{4,28},{8,16},{12,20},{16,8},{20,12},{24,0},{28,4},{1,25},{... | collective-permute-start | bytes 245768 | tf_op jit(solution)/shard_map/ppermute | solution.py:40
  16.2 0.6 collective-permute-start
  16.8 2.3 %collective-permute-done.2 = bf16[64,640]{1,0:T(8,128)(2,1)S(1)} collective-permute-done((bf16[64,640]{1,0:T(8,128)(2,1)S(1)}, bf16[64,640]{1,0:T(8,128)(2,1)S(1)}, u32[]{:S(2)}, u32[]{:S(2)}) %collective-permute-start.2) | collective-permute-done | bytes 81952 | tf_op jit(solution)/shard_map/ppermute | solution.py:40
  19.2 3.9 %collective-permute-done.1 = bf16[64,640]{1,0:T(8,128)(2,1)S(1)} collective-permute-done((bf16[64,640]{1,0:T(8,128)(2,1)S(1)}, bf16[64,640]{1,0:T(8,128)(2,1)S(1)}, u32[]{:S(2)}, u32[]{:S(2)}) %collective-permute-start.1) | collective-permute-done | bytes 81952 | tf_op jit(solution)/shard_map/ppermute | solution.py:40
  23.1 1.6 %collective-permute-start.3 = (bf16[4,64,640]{2,1,0:T(8,128)(2,1)S(1)}, bf16[4,64,640]{2,1,0:T(8,128)(2,1)S(1)}, u32[]{:S(2)}, u32[]{:S(2)}) collective-permute-start(bf16[4,64,640]{2,1,0:T(8,128)(2,1)S(1)} %pad_maximum_fusion.3.mine_ref), channel_id=1, source_target_pairs={{0,4},{4,0},{8,12},{12,8},{16,20},{20,16},{24,28},{28,24},{1,5},{5... | collective-permute-start | bytes 983048 | tf_op jit(solution)/shard_map/ppermute | solution.py:40
  24.8 0.7 pad_maximum_fusion.5
  25.6 0.9 concatenate.48
  26.5 0.1 concatenate.47
  26.7 5.5 %collective-permute-done.3.mine_ref = bf16[4,64,640]{2,1,0:T(8,128)(2,1)S(1)} collective-permute-done((bf16[4,64,640]{2,1,0:T(8,128)(2,1)S(1)}, bf16[4,64,640]{2,1,0:T(8,128)(2,1)S(1)}, u32[]{:S(2)}, u32[]{:S(2)}) %collective-permute-start.3) | collective-permute-done | bytes 327712 | tf_op jit(solution)/shard_map/ppermute | solution.py:40
  32.1 0.8 pad_maximum_fusion.4.q_ref
  32.9 0.6 pad_add_fusion.where_ref
  33.5 0.8 pad_maximum_fusion.2.other_ref
  34.3 4.0 %shard_map.191 = (f32[4,128,128]{2,1,0:T(8,128)}, f32[4,128,128]{2,1,0:T(8,128)}, f32[4,128,128]{2,1,0:T(8,128)}) custom-call(s32[2]{0:T(128)} %pad_add_fusion.where_ref, bf16[4,128,256]{2,1,0:T(8,128)(2,1)} %pad_maximum_fusion.4.q_ref, bf16[4,64,640]{2,1,0:T(8,128)(2,1)} %copy-done.7, bf16[4,64,640]{2,1,0:T(8,128)(2,1)} %pad_maximum_fusion.2.other_ref, ...), custom_call_target="tpu_custom_call" | custom-call | flops 1000000000 | tf_op jit(solution)/shard_map/pallas_call | solution.py:267
  38.3 0.7 copy-done.6
  39.0 5.6 %shard_map.192 = (bf16[2,128,512]{2,1,0:T(8,128)(2,1)}, bf16[2,128,512]{2,1,0:T(8,128)(2,1)}) custom-call(s32[2]{0:T(128)} %pad_add_fusion.where_ref, bf16[4,128,256]{2,1,0:T(8,128)(2,1)} %pad_maximum_fusion.4.q_ref, bf16[4,64,640]{2,1,0:T(8,128)(2,1)} %copy-done.5, bf16[4,64,640]{2,1,0:T(8,128)(2,1)} %copy-done.6, bf16[512,256]{1,0:T(8,128)(2,1)} %kw_ref.3, ...), custom_call_target="tpu_custom_call" | custom-call | flops 1000000000 | tf_op jit(solution)/shard_map/pallas_call | solution.py:269
  44.6 0.5 collective-permute-start.6
  45.1 1.4 %collective-permute-done.6 = bf16[2,128,512]{2,1,0:T(8,128)(2,1)S(1)} collective-permute-done((bf16[2,128,512]{2,1,0:T(8,128)(2,1)}, bf16[2,128,512]{2,1,0:T(8,128)(2,1)S(1)}, u32[]{:S(2)}, u32[]{:S(2)}) %collective-permute-start.6) | collective-permute-done | bytes 262176 | tf_op jit(solution)/shard_map/ppermute | solution.py:40
  46.5 1.0 select_convert_fusion.1
  47.5 1.7 %collective-permute-start.7 = (bf16[1,128,512]{2,1,0:T(8,128)(2,1)S(1)}, bf16[1,128,512]{2,1,0:T(8,128)(2,1)S(1)}, u32[]{:S(2)}, u32[]{:S(2)}) collective-permute-start(bf16[1,128,512]{2,1,0:T(8,128)(2,1)S(1)} %select_convert_fusion.1), channel_id=1, source_target_pairs={{0,2},{1,3},{2,0},{3,1},{4,6},{5,7},{6,4},{7,5},{8,10},{9,11},{10,... | collective-permute-start | bytes 393224 | tf_op jit(solution)/shard_map/ppermute | solution.py:40
  49.2 0.6 gather_fusion
  49.9 0.9 slice.173
  50.8 0.1 copy.56
  51.0 0.1 copy.54
  51.1 0.9 slice.174
  52.2 0.9 slice.172
  53.2 0.2 collective-permute-done.7
  53.4 1.0 fusion.34
  54.4 0.9 convolution_convert_fusion
  55.3 4.2 %all-to-all-start = ((bf16[8,32,512]{2,1,0:T(8,128)(2,1)}), bf16[8,32,512]{2,1,0:T(8,128)(2,1)S(1)}, u32[]{:S(2)}, u32[]{:S(2)}) async-start(bf16[8,32,512]{2,1,0:T(8,128)(2,1)} %bitcast.14), calls=%async_computation | async-start | bytes 524288 | tf_op jit(solution)/shard_map/all_to_all | solution.py:306
  59.7 8.8 %all-to-all-done = bf16[8,32,512]{2,1,0:T(8,128)(2,1)S(1)} async-done(((bf16[8,32,512]{2,1,0:T(8,128)(2,1)}), bf16[8,32,512]{2,1,0:T(8,128)(2,1)S(1)}, u32[]{:S(2)}, u32[]{:S(2)}) %all-to-all-start) | async-done | bytes 262176 | tf_op jit(solution)/shard_map/all_to_all | solution.py:306
  68.5 1.2 %collective-permute-start.8 = (bf16[256,512]{1,0:T(8,128)(2,1)S(1)}, bf16[256,512]{1,0:T(8,128)(2,1)S(1)}, u32[]{:S(2)}, u32[]{:S(2)}) collective-permute-start(bf16[256,512]{1,0:T(8,128)(2,1)S(1)} %bitcast.92), channel_id=1, source_target_pairs={{0,2},{1,3},{2,0},{3,1},{4,6},{5,7},{6,4},{7,5},{8,10},{9,11},{10,... | collective-permute-start | bytes 786440 | tf_op jit(solution)/shard_map/ppermute | solution.py:40
  69.7 0.1 fusion.19
  69.8 5.0 %collective-permute-done.8 = bf16[256,512]{1,0:T(8,128)(2,1)S(1)} collective-permute-done((bf16[256,512]{1,0:T(8,128)(2,1)S(1)}, bf16[256,512]{1,0:T(8,128)(2,1)S(1)}, u32[]{:S(2)}, u32[]{:S(2)}) %collective-permute-start.8) | collective-permute-done | bytes 262176 | tf_op jit(solution)/shard_map/ppermute | solution.py:40
  74.8 0.1 fusion.38
  75.0 0.2 fusion.79
  75.3 0.3 copy-done.8
  75.5 0.7 copy-done.9
  76.2 0.3 collective-permute-done.9
  76.5 1.2 %broadcast_select_fusion.9 = (bf16[256,512]{1,0:T(8,128)(2,1)S(1)}, bf16[256,512]{1,0:T(8,128)(2,1)S(1)}, bf16[256,512]{1,0:T(8,128)(2,1)S(1)}, bf16[256,512]{1,0:T(8,128)(2,1)S(1)}) fusion(pred[]{:T(512)S(6)} %eq.95, bf16[256,512]{1,0:T(8,128)(2,1)} %collective-permute-done.9, bf16[256,512]{1,0:T(8,128)(2,1)} %copy-done.8, pred[]{:T(512)S(6)} %eq.106, ...), kind=kLoop, calls=%fused_computation.62 | loop fusion | flops 1048576 | bytes 2097154 | tf_op jit(solution)/shard_map/jit(_where)/select_n | solution.py:317
  77.7 0.3 fusion.1
  78.0 0.4 copy-done.2
  78.6 2.3 %fusion.7 = f32[256,4,128]{2,0,1:T(8,128)} fusion(bf16[1,4,2048,128]{3,2,1,0:T(8,128)(2,1)S(1)} %copy-done.11, f32[2048]{0:T(1024)} %param.32, f32[256]{0:T(256)S(1)} %add_rsqrt_fusion, bf16[256,512]{1,0:T(8,128)(2,1)S(1)} %get-tuple-element.22, bf16[256,512]{1,0:T(8,128)(2,1)S(1)} %get-tuple-element.21, bf16[256,512]{1,0:T(8,128)(2,1)S(1)} %get-tuple-element.20, ...), kind=kOutput, calls=%fused_computation.11 | convolution fusion | flops 542638080 | bytes 3679232 | tf_op jit(solution)/shard_map/rd,edf->ref/dot_general | solution.py:321
  80.9 3.4 %fusion = bf16[256,2048]{1,0:T(8,128)(2,1)S(1)} fusion(bf16[1,4,128,2048]{3,2,1,0:T(8,128)(2,1)S(1)} %copy-done, bf16[1,4,2048,128]{3,2,1,0:T(8,128)(2,1)} %param.38, f32[2048]{0:T(1024)} %param.32, f32[256]{0:T(256)S(1)} %add_rsqrt_fusion, f32[256,4,128]{2,0,1:T(8,128)} %fusion.7, f32[256,4]{0,1:T(4,128)S(1)} %mul.175, bf16[256,512]{1,0:T(8,128)(2,1)} %copy-done.4, ...), kind=kOutput, calls=%fused_computation.4 | convolution fusion | flops 1080950784 | bytes 6829056 | tf_op jit(solution)/shard_map/ref,efd->rd/dot_general | solution.py:324
  84.4 0.2 collective-permute-start.11
  84.6 1.8 %collective-permute-done.11 = bf16[2,256,512]{2,1,0:T(8,128)(2,1)S(1)} collective-permute-done((bf16[2,256,512]{2,1,0:T(8,128)(2,1)S(1)}, bf16[2,256,512]{2,1,0:T(8,128)(2,1)S(1)}, u32[]{:S(2)}, u32[]{:S(2)}) %collective-permute-start.11) | collective-permute-done | bytes 524320 | tf_op jit(solution)/shard_map/ppermute | solution.py:40
  86.4 0.2 fusion.33
  86.6 1.3 %collective-permute-start.12 = (bf16[1,256,512]{2,1,0:T(8,128)(2,1)S(1)}, bf16[1,256,512]{2,1,0:T(8,128)(2,1)S(1)}, u32[]{:S(2)}, u32[]{:S(2)}) collective-permute-start(bf16[1,256,512]{2,1,0:T(8,128)(2,1)S(1)} %fusion.33), channel_id=1, source_target_pairs={{0,2},{1,3},{2,0},{3,1},{4,6},{5,7},{6,4},{7,5},{8,10},{9,11},{10,... | collective-permute-start | bytes 786440 | tf_op jit(solution)/shard_map/ppermute | solution.py:40
  87.8 7.2 %collective-permute-done.12 = bf16[1,256,512]{2,1,0:T(8,128)(2,1)S(1)} collective-permute-done((bf16[1,256,512]{2,1,0:T(8,128)(2,1)S(1)}, bf16[1,256,512]{2,1,0:T(8,128)(2,1)S(1)}, u32[]{:S(2)}, u32[]{:S(2)}) %collective-permute-start.12) | collective-permute-done | bytes 262176 | tf_op jit(solution)/shard_map/ppermute | solution.py:40
  95.0 0.2 fusion.27
  95.2 13.2 %all_to_all.10 = bf16[8,32,512]{2,1,0:T(8,128)(2,1)S(1)} all-to-all(bf16[8,32,512]{2,1,0:T(8,128)(2,1)S(1)} %bitcast.94), channel_id=1, replica_groups=mesh['sp'=8,'tp'=4] {'sp'}, dimensions={0} | all-to-all | bytes 524288 | tf_op jit(solution)/shard_map/all_to_all | solution.py:327
  108.4 0.9 fusion.18
  (51 shorter events, 1.2 us)
Async XLA Ops:
  0.0 80.9 %copy-start = (bf16[1,4,128,2048]{3,2,1,0:T(8,128)(2,1)S(1)}, bf16[1,4,128,2048]{3,2,1,0:T(8,128)(2,1)}, u32[]{:S(2)}) copy-start(bf16[1,4,128,2048]{3,2,1,0:T(8,128)(2,1)} %param.39) | copy-start | bytes 6291460
  0.0 24.7 %copy-start.10 = (bf16[128,384]{1,0:T(8,128)(2,1)S(1)}, bf16[128,384]{1,0:T(8,128)(2,1)}, u32[]{:S(2)}) copy-start(bf16[128,384]{1,0:T(8,128)(2,1)} %param.20) | copy-start | bytes 294916
  11.1 8.1 %collective-permute-start.2 = (bf16[64,640]{1,0:T(8,128)(2,1)S(1)}, bf16[64,640]{1,0:T(8,128)(2,1)S(1)}, u32[]{:S(2)}, u32[]{:S(2)}) collective-permute-start(bf16[64,640]{1,0:T(8,128)(2,1)S(1)} %get-tuple-element.24), channel_id=1, source_target_pairs={{0,24},{4,28},{8,16},{12,20},{16,8},{20,12},{24,0},{28,4},{1,25},{... | collective-permute-start | bytes 245768 | tf_op jit(solution)/shard_map/ppermute | solution.py:40
  16.2 6.9 %collective-permute-start.1 = (bf16[64,640]{1,0:T(8,128)(2,1)S(1)}, bf16[64,640]{1,0:T(8,128)(2,1)S(1)}, u32[]{:S(2)}, u32[]{:S(2)}) collective-permute-start(bf16[64,640]{1,0:T(8,128)(2,1)S(1)} %get-tuple-element.24), channel_id=1, source_target_pairs={{0,16},{4,20},{8,24},{12,28},{16,0},{20,4},{24,8},{28,12},{1,17},{... | collective-permute-start | bytes 245768 | tf_op jit(solution)/shard_map/ppermute | solution.py:40
  16.2 6.9 %collective-permute-start = (bf16[64,640]{1,0:T(8,128)(2,1)S(1)}, bf16[64,640]{1,0:T(8,128)(2,1)S(1)}, u32[]{:S(2)}, u32[]{:S(2)}) collective-permute-start(bf16[64,640]{1,0:T(8,128)(2,1)S(1)} %get-tuple-element.24), channel_id=1, source_target_pairs={{0,8},{4,12},{8,0},{12,4},{16,24},{20,28},{24,16},{28,20},{1,9},{5... | collective-permute-start | bytes 245768 | tf_op jit(solution)/shard_map/ppermute | solution.py:40
  23.1 3.5 %copy-start.7 = (bf16[4,64,640]{2,1,0:T(8,128)(2,1)}, bf16[4,64,640]{2,1,0:T(8,128)(2,1)S(1)}, u32[]{:S(2)}) copy-start(bf16[4,64,640]{2,1,0:T(8,128)(2,1)S(1)} %pad_maximum_fusion.3.mine_ref) | copy-start | bytes 983044
  23.1 9.0 %collective-permute-start.3 = (bf16[4,64,640]{2,1,0:T(8,128)(2,1)S(1)}, bf16[4,64,640]{2,1,0:T(8,128)(2,1)S(1)}, u32[]{:S(2)}, u32[]{:S(2)}) collective-permute-start(bf16[4,64,640]{2,1,0:T(8,128)(2,1)S(1)} %pad_maximum_fusion.3.mine_ref), channel_id=1, source_target_pairs={{0,4},{4,0},{8,12},{12,8},{16,20},{20,16},{24,28},{28,24},{1,5},{5... | collective-permute-start | bytes 983048 | tf_op jit(solution)/shard_map/ppermute | solution.py:40
  25.5 8.0 %collective-permute-start.5 = (bf16[3,64,640]{2,1,0:T(8,128)(2,1)}, bf16[3,64,640]{2,1,0:T(8,128)(2,1)S(1)}, u32[]{:S(2)}, u32[]{:S(2)}) collective-permute-start(bf16[3,64,640]{2,1,0:T(8,128)(2,1)} %pad_maximum_fusion.5), channel_id=1, source_target_pairs={{0,1},{1,0},{2,3},{3,2},{4,5},{5,4},{6,7},{7,6},{8,9},{9,8},{10,11... | collective-permute-start | bytes 737288 | tf_op jit(solution)/shard_map/ppermute | solution.py:40
  32.1 6.2 %copy-start.5 = (bf16[4,64,640]{2,1,0:T(8,128)(2,1)}, bf16[4,64,640]{2,1,0:T(8,128)(2,1)S(1)}, u32[]{:S(2)}) copy-start(bf16[4,64,640]{2,1,0:T(8,128)(2,1)S(1)} %collective-permute-done.3.mine_ref) | copy-start | bytes 983044
  32.1 6.2 %collective-permute-start.4 = (bf16[4,64,640]{2,1,0:T(8,128)(2,1)S(1)}, bf16[4,64,640]{2,1,0:T(8,128)(2,1)S(1)}, u32[]{:S(2)}, u32[]{:S(2)}) collective-permute-start(bf16[4,64,640]{2,1,0:T(8,128)(2,1)S(1)} %collective-permute-done.3.mine_ref), channel_id=1, source_target_pairs={{0,1},{1,0},{2,3},{3,2},{4,5},{5,4},{6,7},{7,6},{8,9},{9,8},{10,11... | collective-permute-start | bytes 983048 | tf_op jit(solution)/shard_map/ppermute | solution.py:40
  38.3 0.7 copy-start.6
  44.6 8.7 %copy-start.1 = (bf16[2,128,512]{2,1,0:T(8,128)(2,1)S(1)}, bf16[2,128,512]{2,1,0:T(8,128)(2,1)}, u32[]{:S(2)}) copy-start(bf16[2,128,512]{2,1,0:T(8,128)(2,1)} %get-tuple-element.13) | copy-start | bytes 786436
  44.6 1.9 %collective-permute-start.6 = (bf16[2,128,512]{2,1,0:T(8,128)(2,1)}, bf16[2,128,512]{2,1,0:T(8,128)(2,1)S(1)}, u32[]{:S(2)}, u32[]{:S(2)}) collective-permute-start(bf16[2,128,512]{2,1,0:T(8,128)(2,1)} %get-tuple-element.14), channel_id=1, source_target_pairs={{0,1},{1,0},{2,3},{3,2},{4,5},{5,4},{6,7},{7,6},{8,9},{9,8},{10,11... | collective-permute-start | bytes 786440 | tf_op jit(solution)/shard_map/ppermute | solution.py:40
  47.5 5.8 %collective-permute-start.7 = (bf16[1,128,512]{2,1,0:T(8,128)(2,1)S(1)}, bf16[1,128,512]{2,1,0:T(8,128)(2,1)S(1)}, u32[]{:S(2)}, u32[]{:S(2)}) collective-permute-start(bf16[1,128,512]{2,1,0:T(8,128)(2,1)S(1)} %select_convert_fusion.1), channel_id=1, source_target_pairs={{0,2},{1,3},{2,0},{3,1},{4,6},{5,7},{6,4},{7,5},{8,10},{9,11},{10,... | collective-permute-start | bytes 393224 | tf_op jit(solution)/shard_map/ppermute | solution.py:40
  55.3 13.2 %all-to-all-start = ((bf16[8,32,512]{2,1,0:T(8,128)(2,1)}), bf16[8,32,512]{2,1,0:T(8,128)(2,1)S(1)}, u32[]{:S(2)}, u32[]{:S(2)}) async-start(bf16[8,32,512]{2,1,0:T(8,128)(2,1)} %bitcast.14), calls=%async_computation | async-start | bytes 524288 | tf_op jit(solution)/shard_map/all_to_all | solution.py:306
  68.5 6.4 %collective-permute-start.8 = (bf16[256,512]{1,0:T(8,128)(2,1)S(1)}, bf16[256,512]{1,0:T(8,128)(2,1)S(1)}, u32[]{:S(2)}, u32[]{:S(2)}) collective-permute-start(bf16[256,512]{1,0:T(8,128)(2,1)S(1)} %bitcast.92), channel_id=1, source_target_pairs={{0,2},{1,3},{2,0},{3,1},{4,6},{5,7},{6,4},{7,5},{8,10},{9,11},{10,... | collective-permute-start | bytes 786440 | tf_op jit(solution)/shard_map/ppermute | solution.py:40
  69.8 5.5 %collective-permute-start.10 = (bf16[256,512]{1,0:T(8,128)(2,1)S(1)}, bf16[256,512]{1,0:T(8,128)(2,1)S(1)}, u32[]{:S(2)}, u32[]{:S(2)}) collective-permute-start(bf16[256,512]{1,0:T(8,128)(2,1)S(1)} %bitcast.93), channel_id=1, source_target_pairs={{0,1},{1,0},{2,3},{3,2},{4,5},{5,4},{6,7},{7,6},{8,9},{9,8},{10,11... | collective-permute-start | bytes 786440 | tf_op jit(solution)/shard_map/ppermute | solution.py:40
  74.8 0.7 copy-start.8
  74.8 1.7 %collective-permute-start.9 = (bf16[256,512]{1,0:T(8,128)(2,1)S(1)}, bf16[256,512]{1,0:T(8,128)(2,1)}, u32[]{:S(2)}, u32[]{:S(2)}) collective-permute-start(bf16[256,512]{1,0:T(8,128)(2,1)S(1)} %collective-permute-done.8), channel_id=1, source_target_pairs={{0,1},{1,0},{2,3},{3,2},{4,5},{5,4},{6,7},{7,6},{8,9},{9,8},{10,11... | collective-permute-start | bytes 786440 | tf_op jit(solution)/shard_map/ppermute | solution.py:40
  75.3 3.3 %copy-start.11 = (bf16[1,4,2048,128]{3,2,1,0:T(8,128)(2,1)S(1)}, bf16[1,4,2048,128]{3,2,1,0:T(8,128)(2,1)}, u32[]{:S(2)}) copy-start(bf16[1,4,2048,128]{3,2,1,0:T(8,128)(2,1)} %param.37) | copy-start | bytes 6291460
  75.5 0.7 copy-start.9
  77.7 0.7 copy-start.2
  77.7 0.8 copy-start.3
  77.7 0.9 copy-start.4
  84.4 2.0 %collective-permute-start.11 = (bf16[2,256,512]{2,1,0:T(8,128)(2,1)S(1)}, bf16[2,256,512]{2,1,0:T(8,128)(2,1)S(1)}, u32[]{:S(2)}, u32[]{:S(2)}) collective-permute-start(bf16[2,256,512]{2,1,0:T(8,128)(2,1)S(1)} %pad_maximum_fusion.1), channel_id=1, source_target_pairs={{0,1},{1,0},{2,3},{3,2},{4,5},{5,4},{6,7},{7,6},{8,9},{9,8},{10,11... | collective-permute-start | bytes 1572872 | tf_op jit(solution)/shard_map/ppermute | solution.py:40
  86.6 8.4 %collective-permute-start.12 = (bf16[1,256,512]{2,1,0:T(8,128)(2,1)S(1)}, bf16[1,256,512]{2,1,0:T(8,128)(2,1)S(1)}, u32[]{:S(2)}, u32[]{:S(2)}) collective-permute-start(bf16[1,256,512]{2,1,0:T(8,128)(2,1)S(1)} %fusion.33), channel_id=1, source_target_pairs={{0,2},{1,3},{2,0},{3,1},{4,6},{5,7},{6,4},{7,5},{8,10},{9,11},{10,... | collective-permute-start | bytes 786440 | tf_op jit(solution)/shard_map/ppermute | solution.py:40
